TPU v7x, 32 devices: a whole 2x2x4 slice. The times are simulated.
32 devices in a mesh: sp: 16 (over z, y, core), tp: 2 (over x).
Axes of the slice: x: 2, y: 2, z: 4, core: 2. Of those that a mesh axis runs over, the one named last changes fastest.
Arguments:
- residual: bfloat16 [2048, 2048], P(('sp', 'tp')), may hold values from -6 to 6
- q_small: bfloat16 [2048, 1024], P('sp', 'tp'), may hold values from -6 to 6
- k_small: bfloat16 [2048, 1024], P('sp', 'tp'), may hold values from -6 to 6
- v_small: bfloat16 [2048, 1024], P('sp', 'tp'), may hold values from -6 to 6
- q_large: bfloat16 [2048, 1024], P('sp', 'tp'), may hold values from -6 to 6
- k_large: bfloat16 [2048, 1024], P('sp', 'tp'), may hold values from -6 to 6
- v_large: bfloat16 [2048, 1024], P('sp', 'tp'), may hold values from -6 to 6
- forget_small: float32 [2048, 16], P('sp', 'tp'), may hold values from 0 to 20
- forget_large: float32 [2048, 8], P('sp', 'tp'), may hold values from 0 to 20
- w_out_small: bfloat16 [1024, 2048], P('tp'), may hold values from -0.125 to 0.125
- w_out_large: bfloat16 [1024, 2048], P('tp'), may hold values from -0.125 to 0.125
- norm_gain: float32 [2048], replicated, may hold values from 0.1 to 1.9
- w_gate: bfloat16 [2048, 4096], P('sp', 'tp'), may hold values from -0.125 to 0.125
- w_up: bfloat16 [2048, 4096], P('sp', 'tp'), may hold values from -0.125 to 0.125
- conv_gate: float32 [3, 4096], P(None, 'tp'), may hold values from -3 to 3
- conv_up: float32 [3, 4096], P(None, 'tp'), may hold values from -3 to 3
- w_down: bfloat16 [4096, 2048], P('tp', 'sp'), may hold values from -0.09375 to 0.09375
Outputs:
- mixed: bfloat16 [2048, 2048], P(('sp', 'tp'))
All inputs are finite; a program needn't handle non-finite values.
Results may differ from a plain program's by a relative error of at most 0.015.
Values may be sent and summed in bfloat16 or wider, within the bound.
A program may use at most 64 MiB of HBM per device.

v0:
```python
import jax
import jax.numpy as jnp
from jax import lax
from jax.sharding import PartitionSpec as P

EPS = 1e-06
NEG = -1e30


def from_behind(block, axis, distance):
    devices = range(lax.axis_size(axis))
    route = [(i - distance, i) for i in devices if i - distance in devices]
    return lax.ppermute(block, axis, route)


def globalize(part, rows):
    heads = part.shape[1]
    blocks = part.reshape(-1, rows, heads)
    totals = blocks[:, -1, :]
    before = jnp.cumsum(totals, axis=0) - totals
    return (blocks + before[:, None, :]).reshape(part.shape)


def attend(carry, keys, values, queries, cum_own, cum_every, qpos):
    top, denom, accum = carry
    count = keys.shape[0]
    heads = queries.shape[1]
    size = queries.shape[2]
    keys = keys.reshape(count, heads, size)
    values = values.reshape(count, heads, size)
    kpos = jnp.arange(count, dtype=jnp.int32)
    scores = jnp.einsum(
        "qhd,khd->qhk", queries, keys, preferred_element_type=jnp.float32
    ) * size ** (-0.5)
    scores = scores + cum_own[:, :, None] - cum_every.T[None, :, :]
    keep = (kpos[None, :] <= qpos[:, None])[:, None, :]
    scores = jnp.where(keep, scores, NEG)
    new_top = jnp.maximum(top, jnp.max(scores, axis=-1))
    weights = jnp.where(keep, jnp.exp(scores - new_top[:, :, None]), 0.0)
    denom = jnp.sum(weights, axis=-1)
    accum = jnp.einsum(
        "qhk,khd->qhd", weights.astype(jnp.bfloat16), values, preferred_element_type=jnp.float32
    )
    return (new_top, denom, accum)


def finish(carry):
    top, denom, accum = carry
    attended = accum / denom[:, :, None]
    normed = attended * lax.rsqrt(jnp.mean(attended * attended, axis=-1, keepdims=True) + EPS)
    return normed.astype(jnp.bfloat16).reshape(attended.shape[0], -1)


def empty_carry(rows, heads, size):
    return (
        jnp.full((rows, heads), NEG, jnp.float32),
        jnp.zeros((rows, heads), jnp.float32),
        jnp.zeros((rows, heads, size), jnp.float32),
    )


def body(
    residual,
    q_small,
    k_small,
    v_small,
    q_large,
    k_large,
    v_large,
    forget_small,
    forget_large,
    w_out_small,
    w_out_large,
    norm_gain,
    w_gate,
    w_up,
    conv_gate,
    conv_up,
    w_down,
):
    rows = q_small.shape[0]
    offset = lax.axis_index("sp") * rows
    qpos = offset + jnp.arange(rows, dtype=jnp.int32)
    gathered = (
        lax.all_gather(w_gate, "sp", axis=0, tiled=True),
        lax.all_gather(w_up, "sp", axis=0, tiled=True),
        lax.all_gather(w_down, "sp", axis=1, tiled=True),
    )
    local_small = jnp.cumsum(jax.nn.log_sigmoid(forget_small), axis=0)
    local_large = jnp.cumsum(jax.nn.log_sigmoid(forget_large), axis=0)
    part_small, part_large = (
        lax.all_gather(local_small, "sp", axis=0, tiled=True),
        lax.all_gather(local_large, "sp", axis=0, tiled=True),
    )
    every_small = globalize(part_small, rows)
    every_large = globalize(part_large, rows)
    cum_small = lax.dynamic_slice_in_dim(every_small, offset, rows, 0)
    cum_large = lax.dynamic_slice_in_dim(every_large, offset, rows, 0)
    heads_small = forget_small.shape[1]
    heads_large = forget_large.shape[1]
    queries_small = q_small.reshape(rows, heads_small, -1)
    queries_large = q_large.reshape(rows, heads_large, -1)
    start_carry = (
        empty_carry(rows, heads_small, queries_small.shape[2]),
        empty_carry(rows, heads_large, queries_large.shape[2]),
    )
    keys_s = lax.all_gather(k_small, "sp", axis=0, tiled=True)
    values_s = lax.all_gather(v_small, "sp", axis=0, tiled=True)
    keys_l = lax.all_gather(k_large, "sp", axis=0, tiled=True)
    values_l = lax.all_gather(v_large, "sp", axis=0, tiled=True)
    small = attend(start_carry[0], keys_s, values_s, queries_small, cum_small, every_small, qpos)
    large = attend(start_carry[1], keys_l, values_l, queries_large, cum_large, every_large, qpos)
    normed_small = finish(small)
    normed_large = finish(large)
    first_part = jnp.dot(normed_small, w_out_small, preferred_element_type=jnp.float32)
    projected = lax.psum_scatter(
        (
            first_part + jnp.dot(normed_large, w_out_large, preferred_element_type=jnp.float32)
        ).astype(jnp.bfloat16),
        "tp",
        scatter_dimension=0,
        tiled=True,
    ).astype(jnp.float32)
    first = residual.astype(jnp.float32) + projected
    normal = (
        first * lax.rsqrt(jnp.mean(first * first, axis=-1, keepdims=True) + EPS) * norm_gain
    ).astype(jnp.bfloat16)
    gate_full, up_full, down_full = gathered
    piece = lax.all_gather(normal, "tp", axis=0, tiled=True)
    gate_part = jnp.dot(piece, gate_full, preferred_element_type=jnp.float32).astype(jnp.bfloat16)
    up_part = jnp.dot(piece, up_full, preferred_element_type=jnp.float32).astype(jnp.bfloat16)
    both = jnp.concatenate([gate_part, up_part], axis=1)
    width = both.shape[0]
    rim = from_behind(both[width - 2 :], "sp", 1)
    extended = jnp.concatenate([rim, both], axis=0).astype(jnp.float32)
    taps = jnp.concatenate([conv_gate, conv_up], axis=1)
    conv = (
        taps[0] * extended[0:width]
        + taps[1] * extended[1 : width + 1]
        + taps[2] * extended[2 : width + 2]
    )
    half = gate_full.shape[1]
    hidden = (jax.nn.silu(conv[:, :half]) * conv[:, half:]).astype(jnp.bfloat16)
    mixed = first + lax.psum_scatter(
        jnp.dot(hidden, down_full, preferred_element_type=jnp.float32).astype(jnp.bfloat16),
        "tp",
        scatter_dimension=0,
        tiled=True,
    ).astype(jnp.float32)
    return mixed.astype(jnp.bfloat16)


def solution(mesh):
    placed = (
        P(("sp", "tp"), None),
        P("sp", "tp"),
        P("sp", "tp"),
        P("sp", "tp"),
        P("sp", "tp"),
        P("sp", "tp"),
        P("sp", "tp"),
        P("sp", "tp"),
        P("sp", "tp"),
        P("tp", None),
        P("tp", None),
        P(),
        P("sp", "tp"),
        P("sp", "tp"),
        P(None, "tp"),
        P(None, "tp"),
        P("tp", "sp"),
    )
    return jax.shard_map(
        body, mesh=mesh, in_specs=placed, out_specs=P(("sp", "tp"), None), check_vma=False
    )
```

profile of v0, /device:TPU:0, one launch (start us, length us, event | category | flops | bytes accessed | tf_op | source)
XLA Modules:
  0.0 472.0 jit_solution(16428870450614130786)
XLA Ops:
  11.4 27.1 %all_gather.34 = f32[2048,4]{1,0:T(8,128)S(1)} all-gather(f32[128,4]{1,0:T(8,128)S(1)} %reduce_window_sum.46), channel_id=1, replica_groups=mesh['sp'=16,'tp'=2] {'sp'}, dimensions={0}, use_global_device_ids=true | all-gather | bytes 34816 | tf_op jit(solution)/shard_map/all_gather | solution.py:93
  38.8 24.5 %all_gather.31 = f32[2048,8]{1,0:T(8,128)S(1)} all-gather(f32[128,8]{1,0:T(8,128)S(1)} %reduce_window_sum.44), channel_id=1, replica_groups=mesh['sp'=16,'tp'=2] {'sp'}, dimensions={0}, use_global_device_ids=true | all-gather | bytes 69632 | tf_op jit(solution)/shard_map/all_gather | solution.py:92
  67.7 4.0 copy.52
  71.7 31.4 %all-gather.8.cloned.1.call-done = bf16[2048,512]{1,0:T(8,128)(2,1)} async-done(((bf16[128,512]{1,0:T(8,128)(2,1)}), bf16[2048,512]{1,0:T(8,128)(2,1)}) %all-gather.8.cloned.1.call-update) | async-done | bytes 2097168 | tf_op jit(solution)/shard_map/all_gather | solution.py:107
  103.0 4.0 copy.35
  107.0 38.0 %all-gather.12.cloned.1.call-done = bf16[2048,512]{0,1:T(8,128)(2,1)} async-done(((bf16[128,512]{0,1:T(8,128)(2,1)}), bf16[2048,512]{0,1:T(8,128)(2,1)}) %all-gather.12.cloned.1.call-update) | async-done | bytes 2097168 | tf_op jit(solution)/shard_map/all_gather | solution.py:109
  145.0 3.7 fusion.47
  151.9 3.4 fusion.4
  155.3 3.2 copy-done.2
  158.5 3.1 fusion.2
  161.6 26.0 %all-gather.10.cloned.1.call-done = bf16[2048,512]{1,0:T(8,128)(2,1)} async-done(((bf16[128,512]{1,0:T(8,128)(2,1)}), bf16[2048,512]{1,0:T(8,128)(2,1)}) %all-gather.10.cloned.1.call-update) | async-done | bytes 2097168 | tf_op jit(solution)/shard_map/all_gather | solution.py:108
  187.6 3.9 copy.42
  191.5 6.6 %multiply_reduce_fusion.2 = (f32[128,8]{0,1:T(8,128)S(1)}, f32[128,8,64]{0,2,1:T(8,128)S(1)}) fusion(f32[128,8]{0,1:T(8,128)S(1)} %fusion.2, bf16[2048,8,64]{0,2,1:T(8,128)(2,1)} %bitcast.82, f32[8,2048,128]{2,1,0:T(8,128)} %copy-done.2, f32[128,8]{0,1:T(8,128)S(1)} %broadcast_maximum_fusion, f32[8,2048]{1,0:T(8,128)S(1)} %copy.41, f32[128,8]{0,1:T(8,128)S(1)} %copy.40, ...), kind=kOutput, calls=%fused_computation.49 | convolution fusion | flops 283311104 | bytes 11091968 | tf_op jit(solution)/shard_map/qhk,khd->qhd/dot_general | solution.py:41
  203.2 11.3 %reduce-scatter.3.cloned.1.call-done = bf16[64,2048]{1,0:T(8,128)(2,1)} async-done(((bf16[128,2048]{1,0:T(8,128)(2,1)}), bf16[64,2048]{1,0:T(8,128)(2,1)}) %reduce-scatter.3.cloned.1.call-update) | async-done | bytes 262160 | tf_op jit(solution)/shard_map/reduce_scatter | solution.py:116
  216.8 8.7 %all_gather.36 = bf16[128,2048]{1,0:T(8,128)(2,1)S(1)} all-gather(bf16[64,2048]{1,0:T(8,128)(2,1)S(1)} %multiply_convert_fusion), channel_id=1, replica_groups=mesh['sp'=16,'tp'=2] {'tp'}, dimensions={0}, use_global_device_ids=true | all-gather | bytes 786432 | tf_op jit(solution)/shard_map/all_gather | solution.py:129
  225.5 65.4 %all-gather.18.cloned.1.call-done = bf16[2048,2048]{1,0:T(8,128)(2,1)} async-done(((bf16[128,2048]{1,0:T(8,128)(2,1)}), bf16[2048,2048]{1,0:T(8,128)(2,1)}) %all-gather.18.cloned.1.call-update) | async-done | bytes 8388624 | tf_op jit(solution)/shard_map/all_gather | solution.py:86
  290.9 4.6 convolution_convert_fusion.1
  295.6 70.4 %all-gather.16.cloned.1.call-done = bf16[2048,2048]{1,0:T(8,128)(2,1)} async-done(((bf16[128,2048]{1,0:T(8,128)(2,1)}), bf16[2048,2048]{1,0:T(8,128)(2,1)}) %all-gather.16.cloned.1.call-update) | async-done | bytes 8388624 | tf_op jit(solution)/shard_map/all_gather | solution.py:85
  366.0 4.6 convolution_convert_fusion.2
  370.7 2.2 collective-permute-start
  373.9 2.0 fusion.15
  375.9 68.5 %all-gather.20.cloned.1.call-done = bf16[2048,2048]{1,0:T(8,128)(2,1)} async-done(((bf16[2048,128]{1,0:T(8,128)(2,1)}), bf16[2048,2048]{1,0:T(8,128)(2,1)}) %all-gather.20.cloned.1.call-update) | async-done | bytes 8388624 | tf_op jit(solution)/shard_map/all_gather | solution.py:87
  444.5 6.3 %convolution_convert_fusion = bf16[128,2048]{1,0:T(8,128)(2,1)} fusion(bf16[2048,2048]{1,0:T(8,128)(2,1)} %all-gather.20.cloned.1.call-done, f32[128,4096]{1,0:T(8,128)} %fusion.15), kind=kOutput, calls=%fused_computation.16 | convolution fusion | flops 1075576832 | bytes 11010048 | tf_op jit(solution)/shard_map/dot_general | solution.py:145
  450.8 13.0 %reduce-scatter.5.cloned.1.call-done = bf16[64,2048]{1,0:T(8,128)(2,1)} async-done(((bf16[128,2048]{1,0:T(8,128)(2,1)}), bf16[64,2048]{1,0:T(8,128)(2,1)}) %reduce-scatter.5.cloned.1.call-update) | async-done | bytes 262160 | tf_op jit(solution)/shard_map/reduce_scatter | solution.py:144
  (86 shorter events, 22.6 us)
Async XLA Ops:
  6.5 191.7 %copy-start = (bf16[512,2048]{1,0:T(8,128)(2,1)S(1)}, bf16[512,2048]{1,0:T(8,128)(2,1)}, u32[]{:S(2)}) copy-start(bf16[512,2048]{1,0:T(8,128)(2,1)} %param.26) | copy-start | bytes 6291460
  6.5 32.0 %copy-start.12 = (f32[128,8]{0,1:T(8,128)S(1)}, f32[128,8]{0,1:T(8,128)}, u32[]{:S(2)}) copy-start(f32[128,8]{0,1:T(8,128)} %param.24) | copy-start | bytes 12292
  6.5 61.1 %all-gather.14.cloned.1.call-start = ((), (), s32[]{:S(2)}) async-start(), calls=%async_computation.5 | async-start | bytes 2228224 | tf_op jit(solution)/shard_map/all_gather | solution.py:110
  7.3 95.8 %all-gather.8.cloned.1.call-start = ((), (), s32[]{:S(2)}) async-start(), calls=%async_computation.2 | async-start | bytes 2228224 | tf_op jit(solution)/shard_map/all_gather | solution.py:107
  8.0 137.0 %all-gather.12.cloned.1.call-start = ((), (), s32[]{:S(2)}) async-start(), calls=%async_computation.4 | async-start | bytes 2228224 | tf_op jit(solution)/shard_map/all_gather | solution.py:109
  9.7 177.8 %all-gather.10.cloned.1.call-start = ((), (), s32[]{:S(2)}) async-start(), calls=%async_computation.3 | async-start | bytes 2228224 | tf_op jit(solution)/shard_map/all_gather | solution.py:108
  10.3 204.2 %reduce-scatter.3.cloned.1.call-start = ((), (), s32[]{:S(2)}) async-start(), calls=%async_computation.6 | async-start | bytes 786432 | tf_op jit(solution)/shard_map/reduce_scatter | solution.py:116
  38.4 28.9 %copy-start.8 = (bf16[128,512]{1,0:T(8,128)(2,1)S(1)}, bf16[128,512]{1,0:T(8,128)(2,1)}, u32[]{:S(2)}) copy-start(bf16[128,512]{1,0:T(8,128)(2,1)} %param.18) | copy-start | bytes 393220
  67.6 77.4 %copy-start.13 = (bf16[128,512]{1,0:T(8,128)(2,1)S(1)}, bf16[128,512]{1,0:T(8,128)(2,1)}, u32[]{:S(2)}) copy-start(bf16[128,512]{1,0:T(8,128)(2,1)} %param.21) | copy-start | bytes 393220
  148.7 1.6 copy-start.7
  150.3 1.6 copy-start.6
  155.2 3.2 copy-start.2
  198.1 1.6 copy-start.5
  198.2 5.0 %copy-start.9 = (f32[3,2048]{1,0:T(4,128)S(1)}, f32[3,2048]{1,0:T(4,128)}, u32[]{:S(2)}) copy-start(f32[3,2048]{1,0:T(4,128)} %param.31) | copy-start | bytes 73732
  198.2 5.0 %copy-start.10 = (f32[3,2048]{1,0:T(4,128)S(1)}, f32[3,2048]{1,0:T(4,128)}, u32[]{:S(2)}) copy-start(f32[3,2048]{1,0:T(4,128)} %param.32) | copy-start | bytes 73732
  198.3 16.3 %copy-start.3 = (bf16[64,2048]{1,0:T(8,128)(2,1)S(1)}, bf16[64,2048]{1,0:T(8,128)(2,1)}, u32[]{:S(2)}) copy-start(bf16[64,2048]{1,0:T(8,128)(2,1)} %param.17) | copy-start | bytes 786436
  198.3 17.5 %copy-start.11 = (f32[2048]{0:T(1024)S(1)}, f32[2048]{0:T(1024)}, u32[]{:S(2)}) copy-start(f32[2048]{0:T(1024)} %param.28) | copy-start | bytes 24580
  201.1 89.8 %all-gather.18.cloned.1.call-start = ((), (), s32[]{:S(2)}) async-start(), calls=%async_computation.8 | async-start | bytes 8912896 | tf_op jit(solution)/shard_map/all_gather | solution.py:86
  201.6 164.3 %all-gather.16.cloned.1.call-start = ((), (), s32[]{:S(2)}) async-start(), calls=%async_computation.7 | async-start | bytes 8912896 | tf_op jit(solution)/shard_map/all_gather | solution.py:85
  202.4 242.1 %all-gather.20.cloned.1.call-start = ((), (), s32[]{:S(2)}) async-start(), calls=%async_computation.9 | async-start | bytes 8912896 | tf_op jit(solution)/shard_map/all_gather | solution.py:87
  203.1 260.6 %reduce-scatter.5.cloned.1.call-start = ((), (), s32[]{:S(2)}) async-start(), calls=%async_computation.10 | async-start | bytes 786432 | tf_op jit(solution)/shard_map/reduce_scatter | solution.py:144
  370.7 3.0 collective-permute-start
  375.9 87.8 %copy-start.4 = (bf16[64,2048]{1,0:T(8,128)(2,1)S(1)}, bf16[64,2048]{1,0:T(8,128)(2,1)}, u32[]{:S(2)}) copy-start(bf16[64,2048]{1,0:T(8,128)(2,1)} %reduce-scatter.3.cloned.1.call-done) | copy-start | bytes 786436
  444.5 21.0 %copy-start.1 = (bf16[512,2048]{1,0:T(8,128)(2,1)S(1)}, bf16[512,2048]{1,0:T(8,128)(2,1)}, u32[]{:S(2)}) copy-start(bf16[512,2048]{1,0:T(8,128)(2,1)} %param.26) | copy-start | bytes 6291460
Sparse Core Ops, SparseCore 0:
  9.5 49.7 all-gather.13
  61.4 41.5 all-gather.7
  105.2 39.7 all-gather.11
  147.0 40.5 all-gather.9
  201.2 13.3 reduce-scatter.2
  216.6 74.2 all-gather.17
  293.1 72.8 all-gather.15
  368.1 76.2 all-gather.19
  450.9 12.7 reduce-scatter.4
where the time goes:
time: 473 us; the launch traced here: 472 us
  waiting for transfers between devices  329 us (70%)
  blocking collectives  60.3 us (13%)
  matrix products  32.2 us (7%)
  local copies, waits for them, and re-layouts  22.4 us (5%)
  between operations  13.5 us (3%)
  other arithmetic  12.6 us (3%)
    all_gather x1, waiting for transfers between devices, body(): lax.all_gather(w_gate, 'sp', axis=0, tiled=True)  70.4 us
    all_gather x1, waiting for transfers between devices, body(): lax.all_gather(w_down, 'sp', axis=1, tiled=True)  68.5 us
    all_gather x1, waiting for transfers between devices, body(): lax.all_gather(w_up, 'sp', axis=0, tiled=True)  65.4 us
    all_gather x1, waiting for transfers between devices, body(): keys_l = lax.all_gather(k_large, 'sp', axis=0, tiled=True)  38 us
    all_gather x1, waiting for transfers between devices, body(): keys_s = lax.all_gather(k_small, 'sp', axis=0, tiled=True)  31.4 us
    all_gather x1, blocking collectives, body(): lax.all_gather(local_large, 'sp', axis=0, tiled=True)  27.1 us
    all_gather x1, waiting for transfers between devices, body(): values_s = lax.all_gather(v_small, 'sp', axis=0, tiled=True)  26 us
    all_gather x1, blocking collectives, body(): lax.all_gather(local_small, 'sp', axis=0, tiled=True)  24.5 us
  transfers between devices with their start and end apart: 10, of which 9 were waited for; matrix products, arithmetic and copies ran while one was open for 9% of the time, Pallas kernels for 0%

commit v1 on v0

--- a/solution.py
+++ b/solution.py
@@ -105,8 +105,11 @@
         empty_carry(rows, heads_large, queries_large.shape[2]),
     )
     keys_s = lax.all_gather(k_small, "sp", axis=0, tiled=True)
-    values_s = lax.all_gather(v_small, "sp", axis=0, tiled=True)
-    keys_l = lax.all_gather(k_large, "sp", axis=0, tiled=True)
+    values_s, keys_l = jnp.split(
+        lax.all_gather(jnp.concatenate([v_small, k_large], 1), "sp", axis=0, tiled=True),
+        [v_small.shape[1]],
+        axis=1,
+    )
     values_l = lax.all_gather(v_large, "sp", axis=0, tiled=True)
     small = attend(start_carry[0], keys_s, values_s, queries_small, cum_small, every_small, qpos)
     large = attend(start_carry[1], keys_l, values_l, queries_large, cum_large, every_large, qpos)

time: 473 us -> 441 us (0.932)
  waiting for transfers between devices: 329 us -> 303 us
    all_gather x2 -> x1, waiting for transfers between devices: 64 us -> 36.6 us  [body(): lax.all_gather(jnp.concatenate([v_small, k_large], 1), 'sp', axis=0, tile...]
  transfers between devices with their start and end apart: 10 -> 9, of which waited for: 9 -> 8; matrix products, arithmetic and copies ran while one was open for 9% -> 8% of each run, Pallas kernels for 0% -> 0%
where the time goes in v1:
time: 441 us; the launch traced here: 440 us
  waiting for transfers between devices  303 us (69%)
  blocking collectives  59.2 us (13%)
  matrix products  30.1 us (7%)
  local copies, waits for them, and re-layouts  18.9 us (4%)
  between operations  13.9 us (3%)
  other arithmetic  12.3 us (3%)
    all_gather x1, waiting for transfers between devices, body(): lax.all_gather(w_gate, 'sp', axis=0, tiled=True)  70.3 us
    all_gather x1, waiting for transfers between devices, body(): lax.all_gather(w_down, 'sp', axis=1, tiled=True)  68.5 us
    all_gather x1, waiting for transfers between devices, body(): lax.all_gather(w_up, 'sp', axis=0, tiled=True)  65.6 us
    all_gather x1, waiting for transfers between devices, body(): lax.all_gather(jnp.concatenate([v_small, k_large], 1), 'sp', axis=0, tile...  36.6 us
    all_gather x1, waiting for transfers between devices, body(): keys_s = lax.all_gather(k_small, 'sp', axis=0, tiled=True)  34.2 us
    all_gather x1, blocking collectives, body(): lax.all_gather(local_large, 'sp', axis=0, tiled=True)  26.9 us
    all_gather x1, blocking collectives, body(): lax.all_gather(local_small, 'sp', axis=0, tiled=True)  23.8 us
    reduce_scatter x1, waiting for transfers between devices, body(): lax.psum_scatter(jnp.dot(hidden, down_full, preferred_element_type=jnp.fl...  13 us
  transfers between devices with their start and end apart: 9, of which 8 were waited for; matrix products, arithmetic and copies ran while one was open for 8% of the time, Pallas kernels for 0%

profile of v1, /device:TPU:0, one launch (start us, length us, event | category | flops | bytes accessed | tf_op | source)
XLA Modules:
  0.0 439.9 jit_solution(10688019138226025006)
XLA Ops:
  11.9 26.9 %all_gather.30 = f32[2048,4]{1,0:T(8,128)S(1)} all-gather(f32[128,4]{1,0:T(8,128)S(1)} %reduce_window_sum.46), channel_id=1, replica_groups=mesh['sp'=16,'tp'=2] {'sp'}, dimensions={0}, use_global_device_ids=true | all-gather | bytes 34816 | tf_op jit(solution)/shard_map/all_gather | solution.py:93
  39.6 23.8 %all_gather.29 = f32[2048,8]{1,0:T(8,128)S(1)} all-gather(f32[128,8]{1,0:T(8,128)S(1)} %reduce_window_sum.44), channel_id=1, replica_groups=mesh['sp'=16,'tp'=2] {'sp'}, dimensions={0}, use_global_device_ids=true | all-gather | bytes 69632 | tf_op jit(solution)/shard_map/all_gather | solution.py:92
  64.2 4.0 copy.52
  68.2 34.2 %all-gather.9.cloned.1.call-done = bf16[2048,512]{1,0:T(8,128)(2,1)} async-done(((bf16[128,512]{1,0:T(8,128)(2,1)}), bf16[2048,512]{1,0:T(8,128)(2,1)}) %all-gather.9.cloned.1.call-update) | async-done | bytes 2097168 | tf_op jit(solution)/shard_map/all_gather | solution.py:107
  102.4 4.0 copy.37
  106.4 6.5 %fusion.4 = (f32[128,8]{0,1:T(8,128)S(1)}, f32[8,2048,128]{2,1,0:T(8,128)S(1)}) fusion(f32[8,2048]{1,0:T(8,128)S(1)} %copy.43, f32[128,8]{0,1:T(8,128)S(1)} %copy.42, pred[128,2048]{0,1:T(8,128)(4,1)S(1)} %iota_compare_fusion, bf16[2048,8,64]{0,2,1:T(8,128)(2,1)} %bitcast.83, bf16[128,8,64]{0,2,1:T(8,128)(2,1)S(1)} %bitcast.88), kind=kOutput, calls=%fused_computation.6 | convolution fusion | flops 278920192 | bytes 10952704 | tf_op jit(solution)/shard_map/qhd,khd->qhk/dot_general | solution.py:32
  112.9 3.2 copy-done.2
  116.1 3.1 fusion.2
  119.2 36.6 %all-gather.7.cloned.1.call-done = bf16[2048,1024]{0,1:T(8,128)(2,1)} async-done(((bf16[128,1024]{0,1:T(8,128)(2,1)}), bf16[2048,1024]{0,1:T(8,128)(2,1)}) %all-gather.7.cloned.1.call-update) | async-done | bytes 4194320 | tf_op jit(solution)/shard_map/all_gather | solution.py:109
  155.8 2.5 fusion.46
  158.3 1.8 fusion.48
  163.1 3.3 multiply_reduce_fusion.2
  171.3 10.9 %reduce-scatter.3.cloned.1.call-done = bf16[64,2048]{1,0:T(8,128)(2,1)} async-done(((bf16[128,2048]{1,0:T(8,128)(2,1)}), bf16[64,2048]{1,0:T(8,128)(2,1)}) %reduce-scatter.3.cloned.1.call-update) | async-done | bytes 262160 | tf_op jit(solution)/shard_map/reduce_scatter | solution.py:119
  184.5 8.5 %all_gather.32 = bf16[128,2048]{1,0:T(8,128)(2,1)S(1)} all-gather(bf16[64,2048]{1,0:T(8,128)(2,1)S(1)} %multiply_convert_fusion), channel_id=1, replica_groups=mesh['sp'=16,'tp'=2] {'tp'}, dimensions={0}, use_global_device_ids=true | all-gather | bytes 786432 | tf_op jit(solution)/shard_map/all_gather | solution.py:132
  193.0 65.6 %all-gather.15.cloned.1.call-done = bf16[2048,2048]{1,0:T(8,128)(2,1)} async-done(((bf16[128,2048]{1,0:T(8,128)(2,1)}), bf16[2048,2048]{1,0:T(8,128)(2,1)}) %all-gather.15.cloned.1.call-update) | async-done | bytes 8388624 | tf_op jit(solution)/shard_map/all_gather | solution.py:86
  258.6 4.6 %convolution_convert_fusion.1 = bf16[128,2048]{1,0:T(8,128)(2,1)S(1)} fusion(bf16[128,2048]{1,0:T(8,128)(2,1)S(1)} %all_gather.32, bf16[2048,2048]{1,0:T(8,128)(2,1)} %all-gather.15.cloned.1.call-done), kind=kOutput, calls=%fused_computation.17 | convolution fusion | flops 1074003968 | bytes 9437184 | tf_op jit(solution)/shard_map/dot_general | solution.py:134
  263.2 70.3 %all-gather.13.cloned.1.call-done = bf16[2048,2048]{1,0:T(8,128)(2,1)} async-done(((bf16[128,2048]{1,0:T(8,128)(2,1)}), bf16[2048,2048]{1,0:T(8,128)(2,1)}) %all-gather.13.cloned.1.call-update) | async-done | bytes 8388624 | tf_op jit(solution)/shard_map/all_gather | solution.py:85
  333.5 4.6 %convolution_convert_fusion.2 = bf16[128,2048]{1,0:T(8,128)(2,1)S(1)} fusion(bf16[128,2048]{1,0:T(8,128)(2,1)S(1)} %all_gather.32, bf16[2048,2048]{1,0:T(8,128)(2,1)} %all-gather.13.cloned.1.call-done), kind=kOutput, calls=%fused_computation.18 | convolution fusion | flops 1074003968 | bytes 9437184 | tf_op jit(solution)/shard_map/dot_general | solution.py:133
  338.2 2.2 collective-permute-start
  341.5 2.0 fusion.15
  343.4 68.5 %all-gather.17.cloned.1.call-done = bf16[2048,2048]{1,0:T(8,128)(2,1)} async-done(((bf16[2048,128]{1,0:T(8,128)(2,1)}), bf16[2048,2048]{1,0:T(8,128)(2,1)}) %all-gather.17.cloned.1.call-update) | async-done | bytes 8388624 | tf_op jit(solution)/shard_map/all_gather | solution.py:87
  412.0 6.3 %convolution_convert_fusion = bf16[128,2048]{1,0:T(8,128)(2,1)} fusion(bf16[2048,2048]{1,0:T(8,128)(2,1)} %all-gather.17.cloned.1.call-done, f32[128,4096]{1,0:T(8,128)} %fusion.15), kind=kOutput, calls=%fused_computation.16 | convolution fusion | flops 1075576832 | bytes 11010048 | tf_op jit(solution)/shard_map/dot_general | solution.py:148
  418.3 13.0 %reduce-scatter.5.cloned.1.call-done = bf16[64,2048]{1,0:T(8,128)(2,1)} async-done(((bf16[128,2048]{1,0:T(8,128)(2,1)}), bf16[64,2048]{1,0:T(8,128)(2,1)}) %reduce-scatter.5.cloned.1.call-update) | async-done | bytes 262160 | tf_op jit(solution)/shard_map/reduce_scatter | solution.py:147
  431.3 1.7 add_convert_fusion
  (88 shorter events, 18.0 us)
Async XLA Ops:
  6.5 159.9 %copy-start = (bf16[512,2048]{1,0:T(8,128)(2,1)S(1)}, bf16[512,2048]{1,0:T(8,128)(2,1)}, u32[]{:S(2)}) copy-start(bf16[512,2048]{1,0:T(8,128)(2,1)} %param.26) | copy-start | bytes 6291460
  6.5 32.8 %copy-start.11 = (f32[128,8]{0,1:T(8,128)S(1)}, f32[128,8]{0,1:T(8,128)}, u32[]{:S(2)}) copy-start(f32[128,8]{0,1:T(8,128)} %param.24) | copy-start | bytes 12292
  6.5 57.7 %all-gather.11.cloned.1.call-start = ((), (), s32[]{:S(2)}) async-start(), calls=%async_computation.4 | async-start | bytes 2228224 | tf_op jit(solution)/shard_map/all_gather | solution.py:113
  7.3 95.1 %all-gather.9.cloned.1.call-start = ((), (), s32[]{:S(2)}) async-start(), calls=%async_computation.3 | async-start | bytes 2228224 | tf_op jit(solution)/shard_map/all_gather | solution.py:107
  8.0 147.8 %all-gather.7.cloned.1.call-start = ((), (), s32[]{:S(2)}) async-start(), calls=%async_computation.2 | async-start | bytes 4456448 | tf_op jit(solution)/shard_map/all_gather | solution.py:109
  10.9 171.4 %reduce-scatter.3.cloned.1.call-start = ((), (), s32[]{:S(2)}) async-start(), calls=%async_computation.5 | async-start | bytes 786432 | tf_op jit(solution)/shard_map/reduce_scatter | solution.py:119
  38.8 25.1 %copy-start.7 = (bf16[128,512]{1,0:T(8,128)(2,1)S(1)}, bf16[128,512]{1,0:T(8,128)(2,1)}, u32[]{:S(2)}) copy-start(bf16[128,512]{1,0:T(8,128)(2,1)} %param.18) | copy-start | bytes 393220
  112.9 3.2 copy-start.2
  119.2 39.1 %copy-start.12 = (bf16[128,512]{1,0:T(8,128)(2,1)S(1)}, bf16[128,512]{1,0:T(8,128)(2,1)}, u32[]{:S(2)}) copy-start(bf16[128,512]{1,0:T(8,128)(2,1)} %param.21) | copy-start | bytes 393220
  158.3 4.6 %slice-start = ((s8[8388608]{0:T(1024)(128)(4,1)}), s8[4194304]{0:T(1024)(128)(4,1)S(1)}, s32[]{:S(2)}) async-start(s8[8388608]{0:T(1024)(128)(4,1)} %bitcast.76), calls=%async_computation.10 | async-start | bytes 8388608
  160.2 1.6 copy-start.6
  160.2 2.9 slice-start.1
  166.3 1.6 copy-start.5
  166.4 4.8 %copy-start.8 = (f32[3,2048]{1,0:T(4,128)S(1)}, f32[3,2048]{1,0:T(4,128)}, u32[]{:S(2)}) copy-start(f32[3,2048]{1,0:T(4,128)} %param.31) | copy-start | bytes 73732
  166.4 4.8 %copy-start.9 = (f32[3,2048]{1,0:T(4,128)S(1)}, f32[3,2048]{1,0:T(4,128)}, u32[]{:S(2)}) copy-start(f32[3,2048]{1,0:T(4,128)} %param.32) | copy-start | bytes 73732
  166.5 15.8 %copy-start.3 = (bf16[64,2048]{1,0:T(8,128)(2,1)S(1)}, bf16[64,2048]{1,0:T(8,128)(2,1)}, u32[]{:S(2)}) copy-start(bf16[64,2048]{1,0:T(8,128)(2,1)} %param.17) | copy-start | bytes 786436
  166.5 16.9 %copy-start.10 = (f32[2048]{0:T(1024)S(1)}, f32[2048]{0:T(1024)}, u32[]{:S(2)}) copy-start(f32[2048]{0:T(1024)} %param.28) | copy-start | bytes 24580
  169.3 89.3 %all-gather.15.cloned.1.call-start = ((), (), s32[]{:S(2)}) async-start(), calls=%async_computation.7 | async-start | bytes 8912896 | tf_op jit(solution)/shard_map/all_gather | solution.py:86
  169.9 163.6 %all-gather.13.cloned.1.call-start = ((), (), s32[]{:S(2)}) async-start(), calls=%async_computation.6 | async-start | bytes 8912896 | tf_op jit(solution)/shard_map/all_gather | solution.py:85
  170.4 241.5 %all-gather.17.cloned.1.call-start = ((), (), s32[]{:S(2)}) async-start(), calls=%async_computation.8 | async-start | bytes 8912896 | tf_op jit(solution)/shard_map/all_gather | solution.py:87
  171.2 260.1 %reduce-scatter.5.cloned.1.call-start = ((), (), s32[]{:S(2)}) async-start(), calls=%async_computation.9 | async-start | bytes 786432 | tf_op jit(solution)/shard_map/reduce_scatter | solution.py:147
  338.2 3.0 collective-permute-start
  343.4 87.8 %copy-start.4 = (bf16[64,2048]{1,0:T(8,128)(2,1)S(1)}, bf16[64,2048]{1,0:T(8,128)(2,1)}, u32[]{:S(2)}) copy-start(bf16[64,2048]{1,0:T(8,128)(2,1)} %reduce-scatter.3.cloned.1.call-done) | copy-start | bytes 786436
  412.0 21.0 %copy-start.1 = (bf16[512,2048]{1,0:T(8,128)(2,1)S(1)}, bf16[512,2048]{1,0:T(8,128)(2,1)}, u32[]{:S(2)}) copy-start(bf16[512,2048]{1,0:T(8,128)(2,1)} %param.26) | copy-start | bytes 6291460
Sparse Core Ops, SparseCore 0:
  9.5 50.1 all-gather.10
  61.8 40.5 all-gather.8
  104.5 51.1 all-gather.6
  169.4 12.7 reduce-scatter.2
  184.2 74.2 all-gather.14
  260.6 72.8 all-gather.12
  335.6 76.2 all-gather.16
  418.4 12.7 reduce-scatter.4
